TPU v7x, 256 devices: a whole 4x4x8 slice. The times are simulated.
256 devices in a mesh: fs: 32 (over z, x), tp: 8 (over y, core).
Axes of the slice: x: 4, y: 4, z: 8, core: 2. Of those that a mesh axis runs over, the one named last changes fastest.
Arguments:
- tokens: bfloat16 [32768, 2048], P(('fs', 'tp')), may hold values from -6 to 6
- gate_pre: bfloat16 [32768, 5632], P('fs', 'tp'), may hold values from -6 to 6
- value_pre: bfloat16 [32768, 5632], P('fs', 'tp'), may hold values from -6 to 6
- up_gate_w: bfloat16 [2048, 5632], P('fs', 'tp'), may hold values from -0.078125 to 0.078125
- up_value_w: bfloat16 [2048, 5632], P('fs', 'tp'), may hold values from -0.078125 to 0.078125
- conv_weight: float32 [3, 5632], P(None, 'tp'), may hold values from -3 to 3
- conv_bias: float32 [5632], P('tp'), may hold values from -3 to 3
- hidden_grad: bfloat16 [32768, 5632], P('fs', 'tp'), may hold values from -6 to 6
Outputs:
- input_grad: bfloat16 [32768, 2048], P(('fs', 'tp'))
- up_gate_grad: float32 [2048, 5632], P('fs', 'tp')
- up_value_grad: float32 [2048, 5632], P('fs', 'tp')
- conv_weight_grad: float32 [3, 5632], P(None, 'tp')
- conv_bias_grad: float32 [5632], P('tp')
All inputs are finite; a program needn't handle non-finite values.
Results may differ from a plain program's by a relative error of at most 0.013.
Values may be sent and summed in bfloat16 or wider, within the bound.
No kernel may reach another device: no remote copies, remote signals or barrier semaphores. Data moves between devices by JAX's collectives and lax.ppermute only.
A program may use at most 128 MiB of HBM per device.

v0:
```python
import jax
import jax.numpy as jnp
from jax import lax
from jax.sharding import Mesh
from jax.sharding import PartitionSpec as P

FS = ("fs_0", "fs_1")
FS_TP = ("fs_0", "fs_1", "tp")


def copy_for_each(shard, axis):
    peers = lax.axis_size(axis)
    return lax.all_to_all(
        jnp.broadcast_to(shard[None], (peers, *shard.shape)), axis, 0, 0, tiled=True
    )


def taken_together(shard, axis):
    return copy_for_each(shard, axis).sum(axis=0)


def in_one_piece(arrays, axis, dim, along):
    ends, at = ([], 0)
    for a in arrays[:-1]:
        at += a.shape[along]
        ends.append(at)
    both = jnp.concatenate(arrays, axis=along)
    return tuple(jnp.split(lax.all_gather(both, axis, axis=dim, tiled=True), ends, axis=along))


def summed_rows(subtotal, axes):
    for axis in axes:
        subtotal = lax.psum_scatter(subtotal, axis, scatter_dimension=0, tiled=True)
    return subtotal


def in_blocks(shard, dim, peers):
    lengths = shard.shape
    blocks = shard.reshape(*lengths[:dim], peers, lengths[dim] // peers, *lengths[dim + 1 :])
    return jnp.moveaxis(blocks, dim, 0)


def summed_on_arrival(shard, axis, dim):
    blocks = in_blocks(shard, dim, lax.axis_size(axis))
    arrived = lax.all_to_all(blocks, axis, split_axis=0, concat_axis=0, tiled=True)
    return arrived.astype(jnp.float32).sum(axis=0)


def contract_rows(left, right):
    return lax.dot_general(
        left, right, (((0,), (0,)), ((), ())), preferred_element_type=jnp.float32
    )


def contract_cols(left, right):
    return lax.dot_general(
        left, right, (((1,), (1,)), ((), ())), preferred_element_type=jnp.float32
    )


def on_device(
    tokens, gate_pre, value_pre, up_gate_w, up_value_w, conv_weight, conv_bias, hidden_grad
):
    length = gate_pre.shape[0]
    col_count = gate_pre.shape[1]
    scale = float(length * lax.axis_size(FS)) ** (-0.5)
    gate_float = gate_pre.astype(jnp.float32)
    padded = jnp.pad(gate_float, ((2, 0), (0, 0)))
    gate_conv = (
        conv_bias
        + conv_weight[0] * padded[:length]
        + conv_weight[1] * padded[1 : length + 1]
        + conv_weight[2] * padded[2:]
    )
    active, gelu_back = jax.vjp(jax.nn.gelu, gate_conv)
    grad_float = hidden_grad.astype(jnp.float32)
    value_grad = (grad_float * active).astype(jnp.bfloat16)
    conv_grad = gelu_back(grad_float * value_pre.astype(jnp.float32))[0]
    shifted = jnp.pad(conv_grad, ((0, 2), (0, 0)))
    gate_grad = (
        conv_weight[2] * conv_grad
        + conv_weight[1] * shifted[1 : length + 1]
        + conv_weight[0] * shifted[2:]
    ).astype(jnp.bfloat16)
    conv_terms = jnp.stack(
        [
            jnp.sum(conv_grad * padded[:length], axis=0),
            jnp.sum(conv_grad * padded[1 : length + 1], axis=0),
            jnp.sum(conv_grad * padded[2:], axis=0),
            jnp.sum(conv_grad, axis=0),
        ]
    )
    conv_total = taken_together(conv_terms, FS) * scale
    whole_tokens = lax.all_gather(tokens, "tp", axis=0, tiled=True)
    full_gate, full_value = in_one_piece((up_gate_w, up_value_w), FS, 0, 1)
    joined = summed_rows(
        jnp.concatenate(
            [contract_rows(whole_tokens, gate_grad), contract_rows(whole_tokens, value_grad)],
            axis=1,
        ),
        FS,
    )
    gate_out = joined[:, :col_count] * scale
    value_out = joined[:, col_count:] * scale
    input_grad = summed_on_arrival(
        (contract_cols(gate_grad, full_gate) + contract_cols(value_grad, full_value)).astype(
            jnp.bfloat16
        ),
        "tp",
        0,
    ).astype(jnp.bfloat16)
    return (input_grad, gate_out, value_out, conv_total[:3], conv_total[3])


def solution(mesh):
    finer = Mesh(mesh.devices.reshape(8, 4, mesh.shape["tp"]), ("fs_0", "fs_1", "tp"))
    in_specs = (
        P(FS_TP, None),
        P(FS, "tp"),
        P(FS, "tp"),
        P(FS, "tp"),
        P(FS, "tp"),
        P(None, "tp"),
        P("tp"),
        P(FS, "tp"),
    )
    out_specs = (P(FS_TP, None), P(FS, "tp"), P(FS, "tp"), P(None, "tp"), P("tp"))
    return jax.shard_map(
        on_device, mesh=finer, in_specs=in_specs, out_specs=out_specs, check_vma=False
    )
```

profile of v0, /device:TPU:8, one launch (start us, length us, event | category | flops | bytes accessed | tf_op | source)
XLA Modules:
  0.0 301.7 jit_solution(17411305977214108581)
XLA Ops:
  7.3 0.7 all-gather.5.cloned.1.call-update
  8.0 1.8 pad_maximum_fusion.1
  9.9 1.8 convert_element_type.26
  11.8 6.5 %multiply_reduce_fusion.2 = (f32[704]{0:T(1024)S(1)}, f32[704]{0:T(1024)S(1)}, f32[704]{0:T(1024)S(1)}, f32[704]{0:T(1024)S(1)}, f32[1024,704]{0,1:T(8,128)S(1)}, /*index=5*/f32[1024,704]{0,1:T(8,128)}) fusion(f32[1024,704]{0,1:T(8,128)S(1)} %convert_element_type.26, bf16[1024,704]{0,1:T(8,128)(2,1)S(1)} %copy-done, bf16[1024,704]{0,1:T(8,128)(2,1)S(1)} %copy-done.2, ...), kind=kLoop, calls=%fused_computation.29 | loop fusion | flops 25949440 | bytes 12998656 | tf_op jit(solution)/shard_map/reduce_sum | solution.py:87
  18.3 3.0 %fusion.6 = bf16[1024,704]{0,1:T(8,128)(2,1)} fusion(f32[1024,704]{0,1:T(8,128)S(1)} %get-tuple-element.32, f32[704]{0:T(1024)S(1)} %get-tuple-element.30, f32[704]{0:T(1024)S(1)} %get-tuple-element.31, f32[704]{0:T(1024)S(1)} %get-tuple-element.29), kind=kLoop, calls=%fused_computation.18 | loop fusion | flops 4325376 | bytes 4333824 | tf_op jit(solution)/shard_map/convert_element_type | solution.py:84
  21.4 25.0 %all-gather.5.cloned.1.call-done = bf16[1024,2048]{1,0:T(8,128)(2,1)} async-done(((bf16[128,2048]{1,0:T(8,128)(2,1)}), bf16[1024,2048]{1,0:T(8,128)(2,1)}) %all-gather.5.cloned.1.call-update) | async-done | bytes 4194320 | tf_op jit(solution)/shard_map/all_gather | solution.py:94
  46.4 8.4 %convolution_bitcast_fusion.1 = f32[2048,704]{0,1:T(8,128)} fusion(bf16[1024,704]{0,1:T(8,128)(2,1)} %fusion.6, bf16[1024,2048]{1,0:T(8,128)(2,1)} %all-gather.5.cloned.1.call-done), kind=kOutput, calls=%fused_computation.5 | convolution fusion | flops 2952790016 | bytes 11403264 | tf_op jit(solution)/shard_map/dot_general | solution.py:50
  54.8 5.3 %convolution_bitcast_fusion = f32[2048,704]{0,1:T(8,128)} fusion(bf16[1024,2048]{1,0:T(8,128)(2,1)S(1)} %copy-done.10, bf16[1024,704]{0,1:T(8,128)(2,1)S(1)} %copy-done.4, f32[1024,704]{0,1:T(8,128)S(1)} %copy-done.1), kind=kOutput, calls=%fused_computation.4 | convolution fusion | flops 2960719872 | bytes 14286848 | tf_op jit(solution)/shard_map/dot_general | solution.py:50
  60.1 10.8 %pad_maximum_fusion = f32[2048,1408]{0,1:T(8,128)} fusion(f32[2048,704]{0,1:T(8,128)} %convolution_bitcast_fusion, f32[2048,704]{0,1:T(8,128)} %convolution_bitcast_fusion.1), kind=kLoop, calls=%fused_computation | loop fusion | flops 2883584 | bytes 23068672 | tf_op jit(solution)/shard_map/concatenate | solution.py:97
  71.0 0.8 broadcast_in_dim.2
  71.8 10.0 %all-to-all-start.1 = ((f32[32,4,704]{2,1,0:T(4,128)}), f32[32,4,704]{2,1,0:T(4,128)S(1)}, u32[]{:S(2)}, u32[]{:S(2)}) async-start(f32[32,4,704]{2,1,0:T(4,128)} %broadcast_in_dim.2), calls=%async_computation.2 | async-start | bytes 786432 | tf_op jit(solution)/shard_map/all_to_all | solution.py:13
  81.8 56.8 %all-gather.3.cloned.1.call-done = bf16[2048,1408]{1,0:T(8,128)(2,1)} async-done(((bf16[64,1408]{1,0:T(8,128)(2,1)}), bf16[2048,1408]{1,0:T(8,128)(2,1)}) %all-gather.3.cloned.1.call-update) | async-done | bytes 5767184 | tf_op jit(solution)/shard_map/all_gather | solution.py:28
  138.7 6.0 %fusion.1 = f32[1024,2048]{1,0:T(8,128)S(1)} fusion(bf16[1024,704]{0,1:T(8,128)(2,1)} %fusion.6, bf16[2048,1408]{1,0:T(8,128)(2,1)} %all-gather.3.cloned.1.call-done), kind=kOutput, calls=%fused_computation.13 | convolution fusion | flops 2952790016 | bytes 12976128 | tf_op jit(solution)/shard_map/dot_general | solution.py:56
  144.7 7.6 %add_convert_fusion = bf16[1024,2048]{1,0:T(8,128)(2,1)} fusion(f32[1024,2048]{1,0:T(8,128)S(1)} %fusion.1, bf16[2048,1408]{1,0:T(8,128)(2,1)S(1)} %copy-done.9, bf16[1024,704]{0,1:T(8,128)(2,1)S(1)} %copy-done.5, f32[1024,704]{0,1:T(8,128)S(1)} %copy-done.1), kind=kOutput, calls=%fused_computation.1 | convolution fusion | flops 2964914176 | bytes 20054016 | tf_op jit(solution)/shard_map/dot_general | solution.py:56
  152.3 5.0 %all-to-all-start = ((bf16[8,128,2048]{2,1,0:T(8,128)(2,1)}), bf16[8,128,2048]{2,1,0:T(8,128)(2,1)}, u32[]{:S(2)}, u32[]{:S(2)}) async-start(bf16[8,128,2048]{2,1,0:T(8,128)(2,1)} %bitcast.11), calls=%async_computation | async-start | bytes 8388608 | tf_op jit(solution)/shard_map/all_to_all | solution.py:45
  157.3 105.4 %reduce-scatter.5.cloned.1.call-done = f32[256,1408]{0,1:T(8,128)} async-done(((f32[2048,1408]{0,1:T(8,128)}), f32[256,1408]{0,1:T(8,128)}) %reduce-scatter.5.cloned.1.call-update) | async-done | bytes 1441808 | tf_op jit(solution)/shard_map/reduce_scatter | solution.py:33
  262.6 2.9 copy.22
  265.7 0.6 slice_reduce_fusion
  266.3 3.8 %reduce_sum.57 = bf16[128,2048]{1,0:T(8,128)(2,1)} reduce(bf16[8,128,2048]{2,1,0:T(8,128)(2,1)} %all-to-all-done, bf16[]{:T(256)} %constant.19.clone.1), dimensions={0}, to_apply=%region_0.1 | reduce | flops 1835008 | bytes 4718594 | tf_op jit(solution)/shard_map/reduce_sum | solution.py:46
  270.1 21.8 %reduce-scatter.7.cloned.1.call-done = f32[64,1408]{1,0:T(8,128)} async-done(((f32[256,1408]{1,0:T(8,128)}), f32[64,1408]{1,0:T(8,128)}) %reduce-scatter.7.cloned.1.call-update) | async-done | bytes 360464
  292.0 1.1 fusion.18
  293.1 0.2 copy.25
  293.3 0.8 copy.20
  294.3 0.8 copy.21
  (42 shorter events, 0.6 us)
Async XLA Ops:
  7.2 4.6 %copy-start = (bf16[1024,704]{0,1:T(8,128)(2,1)S(1)}, bf16[1024,704]{0,1:T(8,128)(2,1)}, u32[]{:S(2)}) copy-start(bf16[1024,704]{0,1:T(8,128)(2,1)} %param.9) | copy-start | bytes 4325380
  7.2 4.5 %copy-start.7 = (f32[3,704]{1,0:T(4,128)S(1)}, f32[3,704]{1,0:T(4,128)}, u32[]{:S(2)}) copy-start(f32[3,704]{1,0:T(4,128)} %param.13) | copy-start | bytes 25348
  7.2 4.6 %copy-start.2 = (bf16[1024,704]{0,1:T(8,128)(2,1)S(1)}, bf16[1024,704]{0,1:T(8,128)(2,1)}, u32[]{:S(2)}) copy-start(bf16[1024,704]{0,1:T(8,128)(2,1)} %param.10) | copy-start | bytes 4325380
  7.2 4.6 %copy-start.8 = (f32[704]{0:T(1024)S(1)}, f32[704]{0:T(1024)}, u32[]{:S(2)}) copy-start(f32[704]{0:T(1024)} %param.14) | copy-start | bytes 8452
  7.2 39.2 %all-gather.5.cloned.1.call-start = ((), (), s32[]{:S(2)}) async-start(), calls=%async_computation.5 | async-start | bytes 4718592 | tf_op jit(solution)/shard_map/all_gather | solution.py:94
  7.9 130.7 %all-gather.3.cloned.1.call-start = ((), (), s32[]{:S(2)}) async-start(), calls=%async_computation.4 | async-start | bytes 5947392 | tf_op jit(solution)/shard_map/all_gather | solution.py:28
  9.8 252.8 %reduce-scatter.5.cloned.1.call-start = ((), (), s32[]{:S(2)}) async-start(), calls=%async_computation.6 | async-start | bytes 12976128 | tf_op jit(solution)/shard_map/reduce_scatter | solution.py:33
  9.9 1.9 copy-start.3
  21.4 33.4 %copy-start.1 = (f32[1024,704]{0,1:T(8,128)S(1)}, f32[1024,704]{0,1:T(8,128)}, u32[]{:S(2)}) copy-start(f32[1024,704]{0,1:T(8,128)} %get-tuple-element.33) | copy-start | bytes 8650756
  46.4 8.4 %copy-start.4 = (bf16[1024,704]{0,1:T(8,128)(2,1)S(1)}, bf16[1024,704]{0,1:T(8,128)(2,1)}, u32[]{:S(2)}) copy-start(bf16[1024,704]{0,1:T(8,128)(2,1)} %param.15) | copy-start | bytes 4325380
  46.4 8.4 %copy-start.10 = (bf16[1024,2048]{1,0:T(8,128)(2,1)S(1)}, bf16[1024,2048]{1,0:T(8,128)(2,1)}, u32[]{:S(2)}) copy-start(bf16[1024,2048]{1,0:T(8,128)(2,1)} %all-gather.5.cloned.1.call-done) | copy-start | bytes 12582916
  71.8 80.4 %all-to-all-start.1 = ((f32[32,4,704]{2,1,0:T(4,128)}), f32[32,4,704]{2,1,0:T(4,128)S(1)}, u32[]{:S(2)}, u32[]{:S(2)}) async-start(f32[32,4,704]{2,1,0:T(4,128)} %broadcast_in_dim.2), calls=%async_computation.2 | async-start | bytes 786432 | tf_op jit(solution)/shard_map/all_to_all | solution.py:13
  138.7 6.0 %copy-start.5 = (bf16[1024,704]{0,1:T(8,128)(2,1)S(1)}, bf16[1024,704]{0,1:T(8,128)(2,1)}, u32[]{:S(2)}) copy-start(bf16[1024,704]{0,1:T(8,128)(2,1)} %param.15) | copy-start | bytes 4325380
  138.7 6.0 %copy-start.9 = (bf16[2048,1408]{1,0:T(8,128)(2,1)S(1)}, bf16[2048,1408]{1,0:T(8,128)(2,1)}, u32[]{:S(2)}) copy-start(bf16[2048,1408]{1,0:T(8,128)(2,1)} %all-gather.3.cloned.1.call-done) | copy-start | bytes 17301508
  152.3 114.0 %all-to-all-start = ((bf16[8,128,2048]{2,1,0:T(8,128)(2,1)}), bf16[8,128,2048]{2,1,0:T(8,128)(2,1)}, u32[]{:S(2)}, u32[]{:S(2)}) async-start(bf16[8,128,2048]{2,1,0:T(8,128)(2,1)} %bitcast.11), calls=%async_computation | async-start | bytes 8388608 | tf_op jit(solution)/shard_map/all_to_all | solution.py:45
  157.3 134.7 %reduce-scatter.7.cloned.1.call-start = ((), (), s32[]{:S(2)}) async-start(), calls=%async_computation.7 | async-start | bytes 1802240
  265.7 27.6 %copy-start.6 = (f32[4,704]{1,0:T(4,128)}, f32[4,704]{1,0:T(4,128)S(1)}, u32[]{:S(2)}) copy-start(f32[4,704]{1,0:T(4,128)S(1)} %broadcast_multiply_fusion.2) | copy-start | bytes 33796
Sparse Core Ops, SparseCore 0:
  9.9 36.4 all-gather.4
  49.5 89.0 all-gather.2
  141.2 121.3 reduce-scatter.4
  265.7 26.2 reduce-scatter.6
where the time goes:
time: 302 us
  waiting for transfers between devices  210 us (70%)
  other arithmetic  28 us (9%)
  matrix products  27.3 us (9%)
  starting transfers between devices  15.1 us (5%)
  between operations  14 us (5%)
  local copies, waits for them, and re-layouts  7.54 us (2%)
    reduce_scatter x1, waiting for transfers between devices, summed_rows(): subtotal = lax.psum_scatter(subtotal, axis, scatter_dimension=0, tiled=True)  105 us
    all_gather x1, waiting for transfers between devices, in_one_piece(): lax.all_gather(both, axis, axis=dim, tiled=True)  56.8 us
    all_gather x1, waiting for transfers between devices, on_device(): whole_tokens = lax.all_gather(tokens, 'tp', axis=0, tiled=True)  25 us
    unnamed x5, waiting for transfers between devices  22.5 us
    dot_general x2, matrix products, contract_rows(): lax.dot_general(left, right, (((0,), (0,)), ((), ())), preferred_element_...  13.7 us
    dot_general x2, matrix products, contract_cols(): lax.dot_general(left, right, (((1,), (1,)), ((), ())), preferred_element_...  13.6 us
    concatenate x1, other arithmetic, on_device(): jnp.concatenate([contract_rows(whole_tokens, gate_grad), contract_rows(wh...  10.8 us
    all_to_all x1, starting transfers between devices, copy_for_each(): lax.all_to_all(jnp.broadcast_to(shard[None], (peers, *shard.shape)), axis...  10 us
  transfers between devices with their start and end apart: 6, of which 4 were waited for; matrix products, arithmetic and copies ran while one was open for 20% of the time, Pallas kernels for 0%

commit v1 on v0

--- a/solution.py
+++ b/solution.py
@@ -91,7 +91,12 @@
         ]
     )
     conv_total = taken_together(conv_terms, FS) * scale
-    whole_tokens = lax.all_gather(tokens, "tp", axis=0, tiled=True)
+    ring = [tokens]
+    for hop in range(7):
+        ring.append(lax.ppermute(ring[-1], "tp", [(dev, (dev + 1) % 8) for dev in range(8)]))
+    whole_tokens = jnp.roll(
+        jnp.concatenate(ring[::-1], axis=0), (lax.axis_index("tp") + 1) * ring[0].shape[0], axis=0
+    )
     full_gate, full_value = in_one_piece((up_gate_w, up_value_w), FS, 0, 1)
     joined = summed_rows(
         jnp.concatenate(

time: 302 us -> 277 us (0.917)
  waiting for transfers between devices: 210 us -> 172 us
  starting transfers between devices: 15.1 us -> 24.7 us
  local copies, waits for them, and re-layouts: 7.54 us -> 13 us
    all_gather x1, waiting for transfers between devices: 56.8 us -> 0.02 us  [in_one_piece(): lax.all_gather(both, axis, axis=dim, tiled=True)]
    ppermute x0 -> x7, waiting for transfers between devices: none -> 50.2 us  [on_device(): lax.ppermute(ring[-1], 'tp', [(dev, (dev + 1) % 8) for dev in range(8)])]
    all_gather x1 -> x0, waiting for transfers between devices: 25 us -> none  [on_device(): whole_tokens = lax.all_gather(tokens, 'tp', axis=0, tiled=True)]
    reduce_scatter x1, waiting for transfers between devices: 105 us -> 94 us  [summed_rows(): subtotal = lax.psum_scatter(subtotal, axis, scatter_dimension=0, tiled=True)]
    all_to_all x1, starting transfers between devices: 4.97 us -> 13 us  [summed_on_arrival(): lax.all_to_all(blocks, axis, split_axis=0, concat_axis=0, tiled=True)]
    unnamed x27 -> x60, local copies, waits for them, and re-layouts: 4.96 us -> 10.4 us
    unnamed x5 -> x4, waiting for transfers between devices: 22.5 us -> 25 us
  transfers between devices with their start and end apart: 6 -> 12, of which waited for: 4 -> 10; matrix products, arithmetic and copies ran while one was open for 20% -> 21% of each run, Pallas kernels for 0% -> 0%
where the time goes in v1:
time: 277 us; the launch traced here: 276 us
  waiting for transfers between devices  172 us (62%)
  other arithmetic  26.9 us (10%)
  starting transfers between devices  24.7 us (9%)
  matrix products  24.4 us (9%)
  between operations  16 us (6%)
  local copies, waits for them, and re-layouts  13 us (5%)
    reduce_scatter x1, waiting for transfers between devices, summed_rows(): subtotal = lax.psum_scatter(subtotal, axis, scatter_dimension=0, tiled=True)  94 us
    ppermute x7, waiting for transfers between devices, on_device(): lax.ppermute(ring[-1], 'tp', [(dev, (dev + 1) % 8) for dev in range(8)])  50.2 us
    unnamed x4, waiting for transfers between devices  25 us
    dot_general x2, matrix products, contract_cols(): lax.dot_general(left, right, (((1,), (1,)), ((), ())), preferred_element_...  13.6 us
    all_to_all x1, starting transfers between devices, summed_on_arrival(): lax.all_to_all(blocks, axis, split_axis=0, concat_axis=0, tiled=True)  13 us
    all_to_all x1, starting transfers between devices, copy_for_each(): lax.all_to_all(jnp.broadcast_to(shard[None], (peers, *shard.shape)), axis...  11.5 us
    dot_general x2, matrix products, contract_rows(): lax.dot_general(left, right, (((0,), (0,)), ((), ())), preferred_element_...  10.8 us
    concatenate x1, other arithmetic, on_device(): jnp.concatenate([contract_rows(whole_tokens, gate_grad), contract_rows(wh...  10.7 us
  transfers between devices with their start and end apart: 12, of which 10 were waited for; matrix products, arithmetic and copies ran while one was open for 21% of the time, Pallas kernels for 0%

profile of v1, /device:TPU:8, one launch (start us, length us, event | category | flops | bytes accessed | tf_op | source)
XLA Modules:
  0.0 276.5 jit_solution(14638624689193232796)
XLA Ops:
  8.1 1.7 pad_maximum_fusion.1
  9.9 8.8 %collective-permute-done = bf16[128,2048]{1,0:T(8,128)(2,1)S(1)} collective-permute-done((bf16[128,2048]{1,0:T(8,128)(2,1)}, bf16[128,2048]{1,0:T(8,128)(2,1)S(1)}, u32[]{:S(2)}, u32[]{:S(2)}) %collective-permute-start) | collective-permute-done | bytes 524320 | tf_op jit(solution)/shard_map/ppermute | solution.py:96
  18.7 8.6 %collective-permute-done.1 = bf16[128,2048]{1,0:T(8,128)(2,1)S(1)} collective-permute-done((bf16[128,2048]{1,0:T(8,128)(2,1)S(1)}, bf16[128,2048]{1,0:T(8,128)(2,1)S(1)}, u32[]{:S(2)}, u32[]{:S(2)}) %collective-permute-start.1) | collective-permute-done | bytes 524320 | tf_op jit(solution)/shard_map/ppermute | solution.py:96
  27.3 8.6 %collective-permute-done.2 = bf16[128,2048]{1,0:T(8,128)(2,1)S(1)} collective-permute-done((bf16[128,2048]{1,0:T(8,128)(2,1)S(1)}, bf16[128,2048]{1,0:T(8,128)(2,1)S(1)}, u32[]{:S(2)}, u32[]{:S(2)}) %collective-permute-start.2) | collective-permute-done | bytes 524320 | tf_op jit(solution)/shard_map/ppermute | solution.py:96
  35.9 8.6 %collective-permute-done.3 = bf16[128,2048]{1,0:T(8,128)(2,1)S(1)} collective-permute-done((bf16[128,2048]{1,0:T(8,128)(2,1)S(1)}, bf16[128,2048]{1,0:T(8,128)(2,1)S(1)}, u32[]{:S(2)}, u32[]{:S(2)}) %collective-permute-start.3) | collective-permute-done | bytes 524320 | tf_op jit(solution)/shard_map/ppermute | solution.py:96
  44.5 8.6 %collective-permute-done.4 = bf16[128,2048]{1,0:T(8,128)(2,1)S(1)} collective-permute-done((bf16[128,2048]{1,0:T(8,128)(2,1)S(1)}, bf16[128,2048]{1,0:T(8,128)(2,1)S(1)}, u32[]{:S(2)}, u32[]{:S(2)}) %collective-permute-start.4) | collective-permute-done | bytes 524320 | tf_op jit(solution)/shard_map/ppermute | solution.py:96
  53.2 1.9 convert_element_type.26
  55.2 6.7 %collective-permute-done.5 = bf16[128,2048]{1,0:T(8,128)(2,1)} collective-permute-done((bf16[128,2048]{1,0:T(8,128)(2,1)S(1)}, bf16[128,2048]{1,0:T(8,128)(2,1)}, u32[]{:S(2)}, u32[]{:S(2)}) %collective-permute-start.5) | collective-permute-done | bytes 524320 | tf_op jit(solution)/shard_map/ppermute | solution.py:96
  61.9 6.5 %multiply_reduce_fusion.2 = (f32[704]{0:T(1024)S(1)}, f32[704]{0:T(1024)S(1)}, f32[704]{0:T(1024)S(1)}, f32[704]{0:T(1024)S(1)}, f32[1024,704]{0,1:T(8,128)S(1)}, /*index=5*/f32[1024,704]{0,1:T(8,128)}) fusion(f32[1024,704]{0,1:T(8,128)S(1)} %convert_element_type.26, bf16[1024,704]{0,1:T(8,128)(2,1)S(1)} %copy-done, bf16[1024,704]{0,1:T(8,128)(2,1)S(1)} %copy-done.11, ...), kind=kLoop, calls=%fused_computation.31 | loop fusion | flops 25949440 | bytes 12998656 | tf_op jit(solution)/shard_map/reduce_sum | solution.py:87
  68.5 2.1 fusion.10
  70.8 1.7 constant_dynamic-update-slice_fusion.15
  72.5 1.2 constant_dynamic-update-slice_fusion.14
  76.5 5.0 %fusion = f32[2048,704]{0,1:T(8,128)} fusion(bf16[1024,704]{0,1:T(8,128)(2,1)S(1)} %fusion.10, bf16[2048,2048]{1,0:T(8,128)(2,1)S(1)} %constant_dynamic-update-slice_fusion, s32[]{:T(128)S(6)} %select_n.14), kind=kOutput, calls=%fused_computation.4 | convolution fusion | flops 2952790016 | bytes 11403268 | tf_op jit(solution)/shard_map/dot_general | solution.py:50
  81.4 5.9 %fusion.2 = f32[2048,704]{0,1:T(8,128)} fusion(bf16[2048,2048]{1,0:T(8,128)(2,1)S(1)} %constant_dynamic-update-slice_fusion, s32[]{:T(128)S(6)} %select_n.14, bf16[1024,704]{0,1:T(8,128)(2,1)S(1)} %copy-done.13, f32[1024,704]{0,1:T(8,128)S(1)} %copy-done.1), kind=kOutput, calls=%fused_computation.6 | convolution fusion | flops 2960719872 | bytes 14286852 | tf_op jit(solution)/shard_map/dot_general | solution.py:50
  87.3 10.7 %pad_maximum_fusion = f32[2048,1408]{0,1:T(8,128)} fusion(f32[2048,704]{0,1:T(8,128)} %fusion.2, f32[2048,704]{0,1:T(8,128)} %fusion), kind=kLoop, calls=%fused_computation | loop fusion | flops 2883584 | bytes 23068672 | tf_op jit(solution)/shard_map/concatenate | solution.py:102
  98.9 11.5 %all-to-all-start.1 = ((f32[32,4,704]{2,1,0:T(4,128)}), f32[32,4,704]{2,1,0:T(4,128)S(1)}, u32[]{:S(2)}, u32[]{:S(2)}) async-start(f32[32,4,704]{2,1,0:T(4,128)} %broadcast_in_dim.2), calls=%async_computation.2 | async-start | bytes 786432 | tf_op jit(solution)/shard_map/all_to_all | solution.py:13
  110.4 6.0 %fusion.5 = f32[1024,2048]{1,0:T(8,128)S(1)} fusion(bf16[1024,704]{0,1:T(8,128)(2,1)} %copy-done.15, bf16[2048,1408]{1,0:T(8,128)(2,1)} %all-gather.2.cloned.1.call-done), kind=kOutput, calls=%fused_computation.15 | convolution fusion | flops 2952790016 | bytes 12976128 | tf_op jit(solution)/shard_map/dot_general | solution.py:56
  116.5 7.6 %add_convert_fusion = bf16[1024,2048]{1,0:T(8,128)(2,1)} fusion(f32[1024,2048]{1,0:T(8,128)S(1)} %fusion.5, bf16[2048,1408]{1,0:T(8,128)(2,1)S(1)} %copy-done.19, bf16[1024,704]{0,1:T(8,128)(2,1)S(1)} %copy-done.14, f32[1024,704]{0,1:T(8,128)S(1)} %copy-done.1), kind=kOutput, calls=%fused_computation.1 | convolution fusion | flops 2964914176 | bytes 20054016 | tf_op jit(solution)/shard_map/dot_general | solution.py:56
  124.0 2.3 all-to-all-done.1
  126.3 13.0 %all-to-all-start = ((bf16[8,128,2048]{2,1,0:T(8,128)(2,1)}), bf16[8,128,2048]{2,1,0:T(8,128)(2,1)}, u32[]{:S(2)}, u32[]{:S(2)}) async-start(bf16[8,128,2048]{2,1,0:T(8,128)(2,1)} %bitcast.5), calls=%async_computation | async-start | bytes 8388608 | tf_op jit(solution)/shard_map/all_to_all | solution.py:45
  139.4 94.0 %reduce-scatter.5.cloned.1.call-done = f32[256,1408]{0,1:T(8,128)} async-done(((f32[2048,1408]{0,1:T(8,128)}), f32[256,1408]{0,1:T(8,128)}) %reduce-scatter.5.cloned.1.call-update) | async-done | bytes 1441808 | tf_op jit(solution)/shard_map/reduce_scatter | solution.py:33
  233.3 2.9 %copy.22 = f32[256,1408]{1,0:T(8,128)} copy(f32[256,1408]{0,1:T(8,128)} %reduce-scatter.5.cloned.1.call-done) | data formatting | bytes 2883584
  237.0 3.8 %reduce_sum.57 = bf16[128,2048]{1,0:T(8,128)(2,1)} reduce(bf16[8,128,2048]{2,1,0:T(8,128)(2,1)} %all-to-all-done, bf16[]{:T(256)} %constant.42.clone.1), dimensions={0}, to_apply=%region_0.1 | reduce | flops 1835008 | bytes 4718594 | tf_op jit(solution)/shard_map/reduce_sum | solution.py:46
  240.8 25.0 %reduce-scatter.7.cloned.1.call-done = f32[64,1408]{1,0:T(8,128)} async-done(((f32[256,1408]{1,0:T(8,128)}), f32[64,1408]{1,0:T(8,128)}) %reduce-scatter.7.cloned.1.call-update) | async-done | bytes 360464
  (87 shorter events, 7.9 us)
Async XLA Ops:
  8.0 47.1 %copy-start.17 = (f32[3,704]{1,0:T(4,128)S(1)}, f32[3,704]{1,0:T(4,128)}, u32[]{:S(2)}) copy-start(f32[3,704]{1,0:T(4,128)} %param.13) | copy-start | bytes 25348
  8.0 53.9 %copy-start.18 = (f32[704]{0:T(1024)S(1)}, f32[704]{0:T(1024)}, u32[]{:S(2)}) copy-start(f32[704]{0:T(1024)} %param.14) | copy-start | bytes 8452
  8.0 102.4 %all-gather.2.cloned.1.call-start = ((), (), s32[]{:S(2)}) async-start(), calls=%async_computation.4 | async-start | bytes 5947392 | tf_op jit(solution)/shard_map/all_gather | solution.py:28
  9.8 223.5 %reduce-scatter.5.cloned.1.call-start = ((), (), s32[]{:S(2)}) async-start(), calls=%async_computation.5 | async-start | bytes 12976128 | tf_op jit(solution)/shard_map/reduce_scatter | solution.py:33
  9.9 52.1 %copy-start = (bf16[1024,704]{0,1:T(8,128)(2,1)S(1)}, bf16[1024,704]{0,1:T(8,128)(2,1)}, u32[]{:S(2)}) copy-start(bf16[1024,704]{0,1:T(8,128)(2,1)} %param.9) | copy-start | bytes 4325380
  9.9 52.1 %copy-start.11 = (bf16[1024,704]{0,1:T(8,128)(2,1)S(1)}, bf16[1024,704]{0,1:T(8,128)(2,1)}, u32[]{:S(2)}) copy-start(bf16[1024,704]{0,1:T(8,128)(2,1)} %param.10) | copy-start | bytes 4325380
  9.9 52.1 %copy-start.12 = (bf16[1024,704]{0,1:T(8,128)(2,1)S(1)}, bf16[1024,704]{0,1:T(8,128)(2,1)}, u32[]{:S(2)}) copy-start(bf16[1024,704]{0,1:T(8,128)(2,1)} %param.15) | copy-start | bytes 4325380
  9.9 8.8 %collective-permute-start = (bf16[128,2048]{1,0:T(8,128)(2,1)}, bf16[128,2048]{1,0:T(8,128)(2,1)S(1)}, u32[]{:S(2)}, u32[]{:S(2)}) collective-permute-start(bf16[128,2048]{1,0:T(8,128)(2,1)} %param.8), channel_id=1, source_target_pairs={{0,1},{1,2},{2,3},{3,4},{4,5},{5,6},{6,7},{7,0},{8,9},{9,10},{10,1... | collective-permute-start | bytes 1572872 | tf_op jit(solution)/shard_map/ppermute | solution.py:96
  18.7 8.6 %collective-permute-start.1 = (bf16[128,2048]{1,0:T(8,128)(2,1)S(1)}, bf16[128,2048]{1,0:T(8,128)(2,1)S(1)}, u32[]{:S(2)}, u32[]{:S(2)}) collective-permute-start(bf16[128,2048]{1,0:T(8,128)(2,1)S(1)} %collective-permute-done), channel_id=1, source_target_pairs={{0,1},{1,2},{2,3},{3,4},{4,5},{5,6},{6,7},{7,0},{8,9},{9,10},{10,1... | collective-permute-start | bytes 1572872 | tf_op jit(solution)/shard_map/ppermute | solution.py:96
  27.3 25.8 %copy-start.3 = (bf16[128,2048]{1,0:T(8,128)(2,1)}, bf16[128,2048]{1,0:T(8,128)(2,1)S(1)}, u32[]{:S(2)}) copy-start(bf16[128,2048]{1,0:T(8,128)(2,1)S(1)} %collective-permute-done.1) | copy-start | bytes 1572868
  27.3 8.6 %collective-permute-start.2 = (bf16[128,2048]{1,0:T(8,128)(2,1)S(1)}, bf16[128,2048]{1,0:T(8,128)(2,1)S(1)}, u32[]{:S(2)}, u32[]{:S(2)}) collective-permute-start(bf16[128,2048]{1,0:T(8,128)(2,1)S(1)} %collective-permute-done.1), channel_id=1, source_target_pairs={{0,1},{1,2},{2,3},{3,4},{4,5},{5,6},{6,7},{7,0},{8,9},{9,10},{10,1... | collective-permute-start | bytes 1572872 | tf_op jit(solution)/shard_map/ppermute | solution.py:96
  35.9 17.2 %copy-start.5 = (bf16[128,2048]{1,0:T(8,128)(2,1)}, bf16[128,2048]{1,0:T(8,128)(2,1)S(1)}, u32[]{:S(2)}) copy-start(bf16[128,2048]{1,0:T(8,128)(2,1)S(1)} %collective-permute-done.2) | copy-start | bytes 1572868
  35.9 8.6 %collective-permute-start.3 = (bf16[128,2048]{1,0:T(8,128)(2,1)S(1)}, bf16[128,2048]{1,0:T(8,128)(2,1)S(1)}, u32[]{:S(2)}, u32[]{:S(2)}) collective-permute-start(bf16[128,2048]{1,0:T(8,128)(2,1)S(1)} %collective-permute-done.2), channel_id=1, source_target_pairs={{0,1},{1,2},{2,3},{3,4},{4,5},{5,6},{6,7},{7,0},{8,9},{9,10},{10,1... | collective-permute-start | bytes 1572872 | tf_op jit(solution)/shard_map/ppermute | solution.py:96
  44.5 8.6 %copy-start.7 = (bf16[128,2048]{1,0:T(8,128)(2,1)}, bf16[128,2048]{1,0:T(8,128)(2,1)S(1)}, u32[]{:S(2)}) copy-start(bf16[128,2048]{1,0:T(8,128)(2,1)S(1)} %collective-permute-done.3) | copy-start | bytes 1572868
  44.5 8.6 %collective-permute-start.4 = (bf16[128,2048]{1,0:T(8,128)(2,1)S(1)}, bf16[128,2048]{1,0:T(8,128)(2,1)S(1)}, u32[]{:S(2)}, u32[]{:S(2)}) collective-permute-start(bf16[128,2048]{1,0:T(8,128)(2,1)S(1)} %collective-permute-done.3), channel_id=1, source_target_pairs={{0,1},{1,2},{2,3},{3,4},{4,5},{5,6},{6,7},{7,0},{8,9},{9,10},{10,1... | collective-permute-start | bytes 1572872 | tf_op jit(solution)/shard_map/ppermute | solution.py:96
  53.2 8.7 %copy-start.9 = (bf16[128,2048]{1,0:T(8,128)(2,1)}, bf16[128,2048]{1,0:T(8,128)(2,1)S(1)}, u32[]{:S(2)}) copy-start(bf16[128,2048]{1,0:T(8,128)(2,1)S(1)} %collective-permute-done.4) | copy-start | bytes 1572868
  53.2 8.7 %collective-permute-start.5 = (bf16[128,2048]{1,0:T(8,128)(2,1)S(1)}, bf16[128,2048]{1,0:T(8,128)(2,1)}, u32[]{:S(2)}, u32[]{:S(2)}) collective-permute-start(bf16[128,2048]{1,0:T(8,128)(2,1)S(1)} %collective-permute-done.4), channel_id=1, source_target_pairs={{0,1},{1,2},{2,3},{3,4},{4,5},{5,6},{6,7},{7,0},{8,9},{9,10},{10,1... | collective-permute-start | bytes 1572872 | tf_op jit(solution)/shard_map/ppermute | solution.py:96
  61.9 8.9 %collective-permute-start.6 = (bf16[128,2048]{1,0:T(8,128)(2,1)}, bf16[128,2048]{1,0:T(8,128)(2,1)}, u32[]{:S(2)}, u32[]{:S(2)}) collective-permute-start(bf16[128,2048]{1,0:T(8,128)(2,1)} %collective-permute-done.5), channel_id=1, source_target_pairs={{0,1},{1,2},{2,3},{3,4},{4,5},{5,6},{6,7},{7,0},{8,9},{9,10},{10,1... | collective-permute-start | bytes 1572872 | tf_op jit(solution)/shard_map/ppermute | solution.py:96
  98.9 27.5 %all-to-all-start.1 = ((f32[32,4,704]{2,1,0:T(4,128)}), f32[32,4,704]{2,1,0:T(4,128)S(1)}, u32[]{:S(2)}, u32[]{:S(2)}) async-start(f32[32,4,704]{2,1,0:T(4,128)} %broadcast_in_dim.2), calls=%async_computation.2 | async-start | bytes 786432 | tf_op jit(solution)/shard_map/all_to_all | solution.py:13
  110.4 6.0 %copy-start.14 = (bf16[1024,704]{0,1:T(8,128)(2,1)S(1)}, bf16[1024,704]{0,1:T(8,128)(2,1)}, u32[]{:S(2)}) copy-start(bf16[1024,704]{0,1:T(8,128)(2,1)} %param.15) | copy-start | bytes 4325380
  110.4 6.0 %copy-start.19 = (bf16[2048,1408]{1,0:T(8,128)(2,1)S(1)}, bf16[2048,1408]{1,0:T(8,128)(2,1)}, u32[]{:S(2)}) copy-start(bf16[2048,1408]{1,0:T(8,128)(2,1)} %all-gather.2.cloned.1.call-done) | copy-start | bytes 17301508
  126.3 110.6 %all-to-all-start = ((bf16[8,128,2048]{2,1,0:T(8,128)(2,1)}), bf16[8,128,2048]{2,1,0:T(8,128)(2,1)}, u32[]{:S(2)}, u32[]{:S(2)}) async-start(bf16[8,128,2048]{2,1,0:T(8,128)(2,1)} %bitcast.5), calls=%async_computation | async-start | bytes 8388608 | tf_op jit(solution)/shard_map/all_to_all | solution.py:45
  139.4 126.4 %reduce-scatter.7.cloned.1.call-start = ((), (), s32[]{:S(2)}) async-start(), calls=%async_computation.6 | async-start | bytes 1802240
  236.4 30.8 %copy-start.16 = (f32[4,704]{1,0:T(4,128)}, f32[4,704]{1,0:T(4,128)S(1)}, u32[]{:S(2)}) copy-start(f32[4,704]{1,0:T(4,128)S(1)} %broadcast_multiply_fusion.2) | copy-start | bytes 33796
  (8 other events, 34.3 us)
Sparse Core Ops, SparseCore 0:
  12.0 89.4 all-gather.1
Sparse Core Ops, SparseCore 1:
  98.1 135.2 reduce-scatter.4
  236.4 29.4 reduce-scatter.6
